TPU v7x, 512 devices: a whole 4x8x8 slice. The times are simulated.
512 devices in a mesh: tp: 64 (over z, y), dp: 8 (over x, core).
Axes of the slice: x: 4, y: 8, z: 8, core: 2. Of those that a mesh axis runs over, the one named last changes fastest.
Arguments:
- hidden: bfloat16 [64, 4096], P(None, 'dp'), may hold values from -6 to 6
- norm_gain: float32 [2, 4096], P(None, 'dp'), may hold values from 0.1 to 1.9
- gate_weight: bfloat16 [2, 4096, 8192], P(None, 'dp', 'tp'), may hold values from -0.09375 to 0.09375
- inner_weight: bfloat16 [2, 4096, 8192], P(None, 'dp', 'tp'), may hold values from -0.09375 to 0.09375
- write_weight: bfloat16 [2, 4096, 2048], P(None, 'dp', 'tp'), may hold values from -0.09375 to 0.09375
- read_weight: bfloat16 [2, 4096, 2048], P(None, 'dp', 'tp'), may hold values from -0.09375 to 0.09375
- step_weight: bfloat16 [2, 4096, 128], P(None, 'dp'), may hold values from -0.09375 to 0.09375
- conv_inner: bfloat16 [2, 4, 8192], P(None, None, 'tp'), may hold values from -3 to 3
- conv_write: bfloat16 [2, 4, 2048], P(None, None, 'tp'), may hold values from -3 to 3
- conv_read: bfloat16 [2, 4, 2048], P(None, None, 'tp'), may hold values from -3 to 3
- step_bias: float32 [2, 128], P(None, 'tp'), may hold values from -4 to -1
- decay_log: float32 [2, 128], P(None, 'tp'), may hold values from -3 to 0.5
- skip_gain: float32 [2, 128], P(None, 'tp'), may hold values from 0.1 to 1.9
- group_gain: float32 [2, 8192], P(None, 'tp'), may hold values from 0.1 to 1.9
- out_weight: bfloat16 [2, 8192, 4096], P(None, 'tp', 'dp'), may hold values from -0.4 to 0.4
- state_inner: bfloat16 [2, 64, 3, 8192], P(None, 'dp', None, 'tp'), may hold values from -6 to 6
- state_write: bfloat16 [2, 64, 3, 2048], P(None, 'dp', None, 'tp'), may hold values from -6 to 6
- state_read: bfloat16 [2, 64, 3, 2048], P(None, 'dp', None, 'tp'), may hold values from -6 to 6
- recurrent: float32 [2, 64, 128, 64, 128], P(None, 'dp', 'tp'), may hold values from -1.2 to 1.2, as said below
Outputs:
- out_hidden: bfloat16 [64, 4096], P(None, 'dp')
- next_inner: bfloat16 [2, 64, 3, 8192], P(None, 'dp', None, 'tp')
- next_write: bfloat16 [2, 64, 3, 2048], P(None, 'dp', None, 'tp')
- next_read: bfloat16 [2, 64, 3, 2048], P(None, 'dp', None, 'tp')
- next_recurrent: float32 [2, 64, 128, 64, 128], P(None, 'dp', 'tp')
Inputs may be any that keep to these rules, and one draw needn't show every extreme that they name: recurrent states of order a tenth, with scales that differ between heads.
All inputs are finite; a program needn't handle non-finite values.
Results may differ from a plain program's by a relative error of at most 0.025.
Values may be sent and summed in bfloat16 or wider, within the bound.
No kernel may reach another device: no remote copies, remote signals or barrier semaphores. Data moves between devices by JAX's collectives and lax.ppermute only.
A program may use at most 64 MiB of HBM per device.

v0:
```python
import jax
import jax.numpy as jnp
from jax import lax
from jax.sharding import Mesh
from jax.sharding import PartitionSpec as P

D = 4096
HEADS = 128
GROUPS = 16
DP = ("dp_0", "dp_1")
TP = ("tp_0", "tp_1")
TP_DP = ("tp_0", "tp_1", "dp_0", "dp_1")
eps = 1e-06


def cut_along(shard, dim, size):
    before, after = (shard.shape[:dim], shard.shape[dim + 1 :])
    return jnp.moveaxis(shard.reshape(*before, size, -1, *after), dim, 0)


def summed_on_arrival(shard, axis, dim):
    size = lax.axis_size(axis)
    pieces = lax.all_to_all(cut_along(shard, dim, size), axis, 0, 0, tiled=True)
    return jnp.sum(pieces.astype(jnp.float32), axis=0)


def side_by_side(arrays, axis, dim, along):
    widths = [a.shape[along] for a in arrays]
    both = jnp.concatenate(arrays, axis=along)
    result = summed_on_arrival(both, axis, dim)
    return tuple(jnp.split(result, [sum(widths[:k]) for k in range(1, len(widths))], axis=along))


def gather_turned(arrays, axis, dims):
    turned = [jnp.moveaxis(a, dim, 0) for a, dim in zip(arrays, dims)]
    both = jnp.concatenate([t.reshape(len(t), -1) for t in turned], axis=1)
    result, at, gathered = (lax.all_gather(both, axis, axis=0, tiled=True), 0, [])
    for t, dim in zip(turned, dims):
        share = result[:, at : at + t[0].size].reshape(-1, *t.shape[1:])
        gathered.append(jnp.moveaxis(share, 0, dim))
        at += t[0].size
    return tuple(gathered)


def over_axes(shard, axes):
    for axis in axes:
        shard = lax.psum(shard, axis)
    return shard


def copy_for_each(shard, axis):
    size = lax.axis_size(axis)
    return lax.all_to_all(
        jnp.broadcast_to(shard[None], (size, *shard.shape)), axis, 0, 0, tiled=True
    )


def laid_out(pieces, dim):
    lengths = list(pieces.shape[1:])
    lengths[dim] *= pieces.shape[0]
    return jnp.moveaxis(pieces, 0, dim).reshape(lengths)


def collect(shard, axis, dim):
    pieces = copy_for_each(shard, axis)
    return laid_out(pieces, dim)


def summed_on_arrival_2(shard, axis, dim):
    pieces = cut_along(shard, dim, lax.axis_size(axis))
    arrived = lax.all_to_all(pieces, axis, split_axis=0, concat_axis=0, tiled=True)
    return arrived.sum(axis=0)


def taken_together(shard, axis):
    return copy_for_each(shard, axis).sum(axis=0)


def convolve(state, fresh_row, kernel):
    window = jnp.concatenate([state, fresh_row[:, None, :]], axis=1)
    summed = jnp.sum(window.astype(jnp.float32) * kernel.astype(jnp.float32)[None], axis=1)
    return (jax.nn.silu(summed), window[:, 1:])


def mixer_block(normed, number, weights):
    (
        gate_weight,
        inner_weight,
        write_weight,
        read_weight,
        step_weight,
        conv_inner,
        conv_write,
        conv_read,
        step_bias,
        decay_log,
        skip_gain,
        group_gain,
        out_weight,
        state_inner,
        state_write,
        state_read,
        recurrent,
    ) = weights

    def partial_of(weight):
        return jnp.dot(normed, weight[number], preferred_element_type=jnp.float32).astype(
            jnp.bfloat16
        )

    summed = side_by_side(
        (
            partial_of(gate_weight),
            partial_of(inner_weight),
            partial_of(write_weight),
            partial_of(read_weight),
            partial_of(step_weight),
        ),
        DP,
        0,
        1,
    )
    gate_raw, inner_raw, write_raw, read_raw, step_raw = [
        member.astype(jnp.bfloat16) for member in summed
    ]
    inner_act, next_inner = convolve(state_inner[number], inner_raw, conv_inner[number])
    write_act, next_write = convolve(state_write[number], write_raw, conv_write[number])
    read_act, next_read = convolve(state_read[number], read_raw, conv_read[number])
    write_all, read_all = gather_turned(
        (write_act.astype(jnp.bfloat16), read_act.astype(jnp.bfloat16)), TP, (1, 1)
    )
    heads_here = step_bias.shape[1]
    head_dim = recurrent.shape[3]
    state_dim = recurrent.shape[4]
    rows_here = inner_act.shape[0]
    first_head = lax.axis_index(TP) * heads_here
    group_index = first_head // (HEADS // GROUPS)
    write_grid = write_all.reshape(rows_here, state_dim, GROUPS)
    read_grid = read_all.reshape(rows_here, state_dim, GROUPS)
    write_vec = lax.dynamic_slice_in_dim(write_grid, group_index, 1, 2)[:, :, 0].astype(jnp.float32)
    read_vec = lax.dynamic_slice_in_dim(read_grid, group_index, 1, 2)[:, :, 0].astype(jnp.float32)
    step_own = lax.dynamic_slice_in_dim(step_raw, first_head, heads_here, 1)
    step_size = jax.nn.softplus(step_own.astype(jnp.float32) + step_bias[number][None, :])
    retain = jnp.exp(-step_size * jnp.exp(decay_log[number])[None, :])
    inner_heads = inner_act.reshape(rows_here, heads_here, head_dim)
    updated = (
        retain[:, :, None, None] * recurrent[number]
        + (step_size[:, :, None] * inner_heads)[:, :, :, None] * write_vec[:, None, None, :]
    )
    readout = jnp.einsum("bhpn,bn->bhp", updated, read_vec, precision=lax.Precision.HIGHEST)
    readout = readout + skip_gain[number][None, :, None] * inner_heads
    gated_out = readout.reshape(rows_here, heads_here * head_dim) * jax.nn.silu(
        gate_raw.astype(jnp.float32)
    )
    selector = (jnp.arange(GROUPS) == group_index).astype(jnp.float32)
    totals = over_axes(jnp.sum(gated_out * gated_out, axis=1)[:, None] * selector[None, :], TP)
    group_sum = jnp.sum(totals * selector[None, :], axis=1, keepdims=True)
    group_factor = lax.rsqrt(group_sum / (HEADS // GROUPS * head_dim) + eps)
    group_normed = (gated_out * group_factor * group_gain[number][None, :]).astype(jnp.bfloat16)
    branch = jnp.dot(
        collect(group_normed, DP, 0), out_weight[number], preferred_element_type=jnp.float32
    )
    return (branch, (next_inner, next_write, next_read, updated))


def columns_over(branch):
    return summed_on_arrival_2(branch, TP, 1)


def local(
    hidden,
    norm_gain,
    gate_weight,
    inner_weight,
    write_weight,
    read_weight,
    step_weight,
    conv_inner,
    conv_write,
    conv_read,
    step_bias,
    decay_log,
    skip_gain,
    group_gain,
    out_weight,
    state_inner,
    state_write,
    state_read,
    recurrent,
):
    weights = (
        gate_weight,
        inner_weight,
        write_weight,
        read_weight,
        step_weight,
        conv_inner,
        conv_write,
        conv_read,
        step_bias,
        decay_log,
        skip_gain,
        group_gain,
        out_weight,
        state_inner,
        state_write,
        state_read,
        recurrent,
    )
    wide_in = hidden.astype(jnp.float32)
    squares = taken_together(jnp.sum(wide_in * wide_in, axis=1, keepdims=True), DP)
    normed = (wide_in * lax.rsqrt(squares / D + eps) * norm_gain[0][None, :]).astype(jnp.bfloat16)
    branch, first_states = mixer_block(normed, 0, weights)
    slice_width = hidden.shape[1] // lax.axis_size(TP)
    offset = lax.axis_index(TP) * slice_width
    own_cols = lax.dynamic_slice_in_dim(wide_in, offset, slice_width, 1)
    middle = (own_cols + columns_over(branch)).astype(jnp.bfloat16).astype(jnp.float32)
    squares = over_axes(jnp.sum(middle * middle, axis=1, keepdims=True), TP_DP)
    gain_slice = lax.dynamic_slice_in_dim(norm_gain[1], offset, slice_width, 0)
    normed_part = (middle * lax.rsqrt(squares / D + eps) * gain_slice[None, :]).astype(jnp.bfloat16)
    normed = collect(normed_part, TP, 1)
    branch, second_states = mixer_block(normed, 1, weights)
    result = collect((middle + columns_over(branch)).astype(jnp.bfloat16), TP, 1)
    stacked = [jnp.stack([earlier, later]) for earlier, later in zip(first_states, second_states)]
    return (result, stacked[0], stacked[1], stacked[2], stacked[3])


def solution(mesh):
    finer = Mesh(mesh.devices.reshape(8, 8, 4, 2), ("tp_0", "tp_1", "dp_0", "dp_1"))
    placed = (
        P(None, DP),
        P(None, DP),
        P(None, DP, TP),
        P(None, DP, TP),
        P(None, DP, TP),
        P(None, DP, TP),
        P(None, DP, None),
        P(None, None, TP),
        P(None, None, TP),
        P(None, None, TP),
        P(None, TP),
        P(None, TP),
        P(None, TP),
        P(None, TP),
        P(None, TP, DP),
        P(None, DP, None, TP),
        P(None, DP, None, TP),
        P(None, DP, None, TP),
        P(None, DP, TP, None, None),
    )
    return jax.shard_map(
        local,
        mesh=finer,
        in_specs=placed,
        out_specs=(
            P(None, DP),
            P(None, DP, None, TP),
            P(None, DP, None, TP),
            P(None, DP, None, TP),
            P(None, DP, TP, None, None),
        ),
        check_vma=False,
    )
```

profile of v0, /device:TPU:8, one launch (start us, length us, event | category | flops | bytes accessed | tf_op | source)
XLA Modules:
  0.0 351.3 jit_solution(7885808371134442058)
XLA Ops:
  2.3 4.4 %all-to-all-start = ((f32[8,64,1]{1,2,0:T(1,128)}), f32[8,64,1]{1,2,0:T(1,128)S(1)}, u32[]{:S(2)}, u32[]{:S(2)}) async-start(f32[8,64,1]{1,2,0:T(1,128)} %broadcast_in_dim.24), calls=%async_computation | async-start | bytes 8192 | tf_op jit(solution)/shard_map/all_to_all | solution.py:53
  16.0 3.4 all-to-all-start.1
  19.4 5.5 %all-to-all-done.1 = bf16[8,8,448]{2,1,0:T(8,128)(2,1)S(1)} async-done(((bf16[8,8,448]{2,1,0:T(8,128)(2,1)}), bf16[8,8,448]{2,1,0:T(8,128)(2,1)S(1)}, u32[]{:S(2)}, u32[]{:S(2)}) %all-to-all-start.1) | async-done | bytes 57376 | tf_op jit(solution)/shard_map/all_to_all | solution.py:23
  25.2 56.1 %all-gather = bf16[64,32,16]{1,2,0:T(8,128)(2,1)S(1)} all-gather(bf16[1,32,16]{1,2,0:T(8,128)(2,1)S(1)} %maximum_bitcast_fusion), channel_id=1, replica_groups=mesh['tp_0'=8,'tp_1'=8,'dp_0'=4,'dp_1'=2] {'tp_0','tp_1'}, dimensions={0}, use_global_device_ids=true | all-gather | bytes 66560 | tf_op jit(solution)/shard_map/all_gather | solution.py:37
  84.0 16.0 %psum.56 = f32[8,16]{1,0:T(8,128)S(1)} all-reduce(f32[8,16]{1,0:T(8,128)S(1)} %broadcast_multiply_fusion.3), channel_id=1, replica_groups=mesh['tp_0'=8,'tp_1'=8,'dp_0'=4,'dp_1'=2] {'tp_0'}, use_global_device_ids=true, to_apply=%region_7.8 | all-reduce | flops 128 | bytes 1024 | tf_op jit(solution)/shard_map/psum | solution.py:47
  100.0 15.4 %psum.57 = f32[8,16]{1,0:T(8,128)S(1)} all-reduce(f32[8,16]{1,0:T(8,128)S(1)} %psum.56), channel_id=1, replica_groups=mesh['tp_0'=8,'tp_1'=8,'dp_0'=4,'dp_1'=2] {'tp_1'}, use_global_device_ids=true, to_apply=%region_8.9 | all-reduce | flops 128 | bytes 1024 | tf_op jit(solution)/shard_map/psum | solution.py:47
  119.7 5.1 %all-to-all-done.2 = bf16[8,8,128]{2,1,0:T(8,128)(2,1)S(1)} async-done(((bf16[8,8,128]{2,1,0:T(8,128)(2,1)}), bf16[8,8,128]{2,1,0:T(8,128)(2,1)S(1)}, u32[]{:S(2)}, u32[]{:S(2)}) %all-to-all-start.2) | async-done | bytes 16416 | tf_op jit(solution)/shard_map/all_to_all | solution.py:53
  126.1 8.3 %all-to-all-start.3 = ((f32[64,1,512]{2,1,0:T(1,128)}), f32[64,1,512]{2,1,0:T(1,128)S(1)}, u32[]{:S(2)}, u32[]{:S(2)}) async-start(f32[64,1,512]{2,1,0:T(1,128)} %reshape.185), calls=%async_computation.3 | async-start | bytes 262144 | tf_op jit(solution)/shard_map/all_to_all | solution.py:71
  134.5 11.7 %all-to-all-done.3 = f32[64,1,512]{2,1,0:T(1,128)S(1)} async-done(((f32[64,1,512]{2,1,0:T(1,128)}), f32[64,1,512]{2,1,0:T(1,128)S(1)}, u32[]{:S(2)}, u32[]{:S(2)}) %all-to-all-start.3) | async-done | bytes 131104 | tf_op jit(solution)/shard_map/all_to_all | solution.py:71
  148.0 14.8 %psum.58 = f32[64,1]{0,1:T(1,128)S(1)} all-reduce(f32[64,1]{0,1:T(1,128)S(1)} %bitcast.277), channel_id=1, replica_groups=mesh['tp_0'=8,'tp_1'=8,'dp_0'=4,'dp_1'=2] {'tp_0'}, use_global_device_ids=true, to_apply=%region_12.13 | all-reduce | flops 64 | bytes 512 | tf_op jit(solution)/shard_map/psum | solution.py:47
  162.8 15.4 %psum.59 = f32[64,1]{0,1:T(1,128)S(1)} all-reduce(f32[64,1]{0,1:T(1,128)S(1)} %psum.58), channel_id=1, replica_groups=mesh['tp_0'=8,'tp_1'=8,'dp_0'=4,'dp_1'=2] {'tp_1'}, use_global_device_ids=true, to_apply=%region_13.14 | all-reduce | flops 64 | bytes 512 | tf_op jit(solution)/shard_map/psum | solution.py:47
  178.2 8.9 %psum.60 = f32[64,1]{0,1:T(1,128)S(1)} all-reduce(f32[64,1]{0,1:T(1,128)S(1)} %psum.59), channel_id=1, replica_groups=mesh['tp_0'=8,'tp_1'=8,'dp_0'=4,'dp_1'=2] {'dp_0'}, use_global_device_ids=true, to_apply=%region_14.15 | all-reduce | flops 64 | bytes 512 | tf_op jit(solution)/shard_map/psum | solution.py:47
  190.4 7.7 %all-to-all-start.4 = ((bf16[64,2,256]{2,1,0:T(2,128)(2,1)}), bf16[64,2,256]{2,1,0:T(2,128)(2,1)S(1)}, u32[]{:S(2)}, u32[]{:S(2)}) async-start(bf16[64,2,256]{2,1,0:T(2,128)(2,1)} %reshape.187), calls=%async_computation.4 | async-start | bytes 131072 | tf_op jit(solution)/shard_map/all_to_all | solution.py:53
  198.3 11.2 %all-to-all-done.4 = bf16[64,2,256]{2,1,0:T(2,128)(2,1)S(1)} async-done(((bf16[64,2,256]{2,1,0:T(2,128)(2,1)}), bf16[64,2,256]{2,1,0:T(2,128)(2,1)S(1)}, u32[]{:S(2)}, u32[]{:S(2)}) %all-to-all-start.4) | async-done | bytes 65568 | tf_op jit(solution)/shard_map/all_to_all | solution.py:53
  211.5 3.4 all-to-all-start.5
  214.9 5.5 %all-to-all-done.5 = bf16[8,8,448]{2,1,0:T(8,128)(2,1)S(1)} async-done(((bf16[8,8,448]{2,1,0:T(8,128)(2,1)}), bf16[8,8,448]{2,1,0:T(8,128)(2,1)S(1)}, u32[]{:S(2)}, u32[]{:S(2)}) %all-to-all-start.5) | async-done | bytes 57376 | tf_op jit(solution)/shard_map/all_to_all | solution.py:23
  220.8 47.6 %all-gather.1 = bf16[64,32,16]{1,2,0:T(8,128)(2,1)S(1)} all-gather(bf16[1,32,16]{1,2,0:T(8,128)(2,1)S(1)} %maximum_bitcast_fusion.1), channel_id=1, replica_groups=mesh['tp_0'=8,'tp_1'=8,'dp_0'=4,'dp_1'=2] {'tp_0','tp_1'}, dimensions={0}, use_global_device_ids=true | all-gather | bytes 66560 | tf_op jit(solution)/shard_map/all_gather | solution.py:37
  271.0 14.8 %psum.62 = f32[8,16]{1,0:T(8,128)S(1)} all-reduce(f32[8,16]{1,0:T(8,128)S(1)} %broadcast_multiply_fusion.2), channel_id=1, replica_groups=mesh['tp_0'=8,'tp_1'=8,'dp_0'=4,'dp_1'=2] {'tp_0'}, use_global_device_ids=true, to_apply=%region_21.22 | all-reduce | flops 128 | bytes 1024 | tf_op jit(solution)/shard_map/psum | solution.py:47
  285.8 16.7 %psum.63 = f32[8,16]{1,0:T(8,128)S(1)} all-reduce(f32[8,16]{1,0:T(8,128)S(1)} %psum.62), channel_id=1, replica_groups=mesh['tp_0'=8,'tp_1'=8,'dp_0'=4,'dp_1'=2] {'tp_1'}, use_global_device_ids=true, to_apply=%region_22.23 | all-reduce | flops 128 | bytes 1024 | tf_op jit(solution)/shard_map/psum | solution.py:47
  303.4 3.5 %all-to-all-start.6 = ((bf16[8,8,128]{2,1,0:T(8,128)(2,1)}), bf16[8,8,128]{2,1,0:T(8,128)(2,1)S(1)}, u32[]{:S(2)}, u32[]{:S(2)}) async-start(bf16[8,8,128]{2,1,0:T(8,128)(2,1)} %broadcast_in_dim.34), calls=%async_computation.6 | async-start | bytes 32768 | tf_op jit(solution)/shard_map/all_to_all | solution.py:53
  313.2 6.4 %all-to-all-start.7 = ((f32[64,1,512]{2,1,0:T(1,128)}), f32[64,1,512]{2,1,0:T(1,128)S(1)}, u32[]{:S(2)}, u32[]{:S(2)}) async-start(f32[64,1,512]{2,1,0:T(1,128)} %reshape.189), calls=%async_computation.7 | async-start | bytes 262144 | tf_op jit(solution)/shard_map/all_to_all | solution.py:71
  320.1 11.4 %all-to-all-done.7 = f32[64,1,512]{2,1,0:T(1,128)S(1)} async-done(((f32[64,1,512]{2,1,0:T(1,128)}), f32[64,1,512]{2,1,0:T(1,128)S(1)}, u32[]{:S(2)}, u32[]{:S(2)}) %all-to-all-start.7) | async-done | bytes 131104 | tf_op jit(solution)/shard_map/all_to_all | solution.py:71
  333.5 5.4 %all-to-all-start.8 = ((bf16[64,2,256]{2,1,0:T(2,128)(2,1)}), bf16[64,2,256]{2,1,0:T(2,128)(2,1)S(1)}, u32[]{:S(2)}, u32[]{:S(2)}) async-start(bf16[64,2,256]{2,1,0:T(2,128)(2,1)} %reshape.191), calls=%async_computation.8 | async-start | bytes 131072 | tf_op jit(solution)/shard_map/all_to_all | solution.py:53
  339.9 10.5 %all-to-all-done.8 = bf16[64,2,256]{2,1,0:T(2,128)(2,1)S(1)} async-done(((bf16[64,2,256]{2,1,0:T(2,128)(2,1)}), bf16[64,2,256]{2,1,0:T(2,128)(2,1)S(1)}, u32[]{:S(2)}, u32[]{:S(2)}) %all-to-all-start.8) | async-done | bytes 65568 | tf_op jit(solution)/shard_map/all_to_all | solution.py:53
  (169 shorter events, 40.9 us)
Async XLA Ops:
  2.3 4.4 %copy-start.14 = (f32[2,2]{1,0:T(2,128)S(1)}, f32[2,2]{1,0:T(2,128)}, u32[]{:S(2)}) copy-start(f32[2,2]{1,0:T(2,128)} %param.31) | copy-start | bytes 52
  2.3 4.5 %copy-start.10 = (f32[2,512]{1,0:T(2,128)S(1)}, f32[2,512]{1,0:T(2,128)}, u32[]{:S(2)}) copy-start(f32[2,512]{1,0:T(2,128)} %param.20) | copy-start | bytes 12292
  2.3 4.5 %copy-start.11 = (bf16[2,4,128]{2,1,0:T(4,128)(2,1)S(1)}, bf16[2,4,128]{2,1,0:T(4,128)(2,1)}, u32[]{:S(2)}) copy-start(bf16[2,4,128]{2,1,0:T(4,128)(2,1)} %param.26) | copy-start | bytes 6148
  2.3 9.6 %all-to-all-start = ((f32[8,64,1]{1,2,0:T(1,128)}), f32[8,64,1]{1,2,0:T(1,128)S(1)}, u32[]{:S(2)}, u32[]{:S(2)}) async-start(f32[8,64,1]{1,2,0:T(1,128)} %broadcast_in_dim.24), calls=%async_computation | async-start | bytes 8192 | tf_op jit(solution)/shard_map/all_to_all | solution.py:53
  6.7 1.4 copy-start.7
  8.2 0.7 copy-start.9
  8.2 0.7 copy-start.16
  8.2 0.7 copy-start.17
  8.2 0.7 copy-start.15
  8.2 3.8 %copy-start.6 = (bf16[2,512,32]{1,2,0:T(8,128)(2,1)S(1)}, bf16[2,512,32]{1,2,0:T(8,128)(2,1)}, u32[]{:S(2)}) copy-start(bf16[2,512,32]{1,2,0:T(8,128)(2,1)} %param.24) | copy-start | bytes 196612
  11.9 0.8 copy-start.5
  12.0 1.2 copy-start.3
  13.0 1.0 copy-start.2
  14.0 0.9 copy-start.4
  16.0 8.9 %all-to-all-start.1 = ((bf16[8,8,448]{2,1,0:T(8,128)(2,1)}), bf16[8,8,448]{2,1,0:T(8,128)(2,1)S(1)}, u32[]{:S(2)}, u32[]{:S(2)}) async-start(bf16[8,8,448]{2,1,0:T(8,128)(2,1)} %bitcast.6), calls=%async_computation.1 | async-start | bytes 131072 | tf_op jit(solution)/shard_map/all_to_all | solution.py:23
  81.3 1.5 copy-start
  82.8 36.8 %copy-start.1 = (bf16[2,128,512]{2,1,0:T(8,128)(2,1)S(1)}, bf16[2,128,512]{2,1,0:T(8,128)(2,1)}, u32[]{:S(2)}) copy-start(bf16[2,128,512]{2,1,0:T(8,128)(2,1)} %param.33) | copy-start | bytes 786436
  116.2 8.6 %all-to-all-start.2 = ((bf16[8,8,128]{2,1,0:T(8,128)(2,1)}), bf16[8,8,128]{2,1,0:T(8,128)(2,1)S(1)}, u32[]{:S(2)}, u32[]{:S(2)}) async-start(bf16[8,8,128]{2,1,0:T(8,128)(2,1)} %broadcast_in_dim.28), calls=%async_computation.2 | async-start | bytes 32768 | tf_op jit(solution)/shard_map/all_to_all | solution.py:53
  126.1 20.2 %all-to-all-start.3 = ((f32[64,1,512]{2,1,0:T(1,128)}), f32[64,1,512]{2,1,0:T(1,128)S(1)}, u32[]{:S(2)}, u32[]{:S(2)}) async-start(f32[64,1,512]{2,1,0:T(1,128)} %reshape.185), calls=%async_computation.3 | async-start | bytes 262144 | tf_op jit(solution)/shard_map/all_to_all | solution.py:71
  190.4 19.0 %all-to-all-start.4 = ((bf16[64,2,256]{2,1,0:T(2,128)(2,1)}), bf16[64,2,256]{2,1,0:T(2,128)(2,1)S(1)}, u32[]{:S(2)}, u32[]{:S(2)}) async-start(bf16[64,2,256]{2,1,0:T(2,128)(2,1)} %reshape.187), calls=%async_computation.4 | async-start | bytes 131072 | tf_op jit(solution)/shard_map/all_to_all | solution.py:53
  211.5 8.9 %all-to-all-start.5 = ((bf16[8,8,448]{2,1,0:T(8,128)(2,1)}), bf16[8,8,448]{2,1,0:T(8,128)(2,1)S(1)}, u32[]{:S(2)}, u32[]{:S(2)}) async-start(bf16[8,8,448]{2,1,0:T(8,128)(2,1)} %bitcast.45), calls=%async_computation.5 | async-start | bytes 131072 | tf_op jit(solution)/shard_map/all_to_all | solution.py:23
  303.4 8.6 %all-to-all-start.6 = ((bf16[8,8,128]{2,1,0:T(8,128)(2,1)}), bf16[8,8,128]{2,1,0:T(8,128)(2,1)S(1)}, u32[]{:S(2)}, u32[]{:S(2)}) async-start(bf16[8,8,128]{2,1,0:T(8,128)(2,1)} %broadcast_in_dim.34), calls=%async_computation.6 | async-start | bytes 32768 | tf_op jit(solution)/shard_map/all_to_all | solution.py:53
  313.2 18.3 %all-to-all-start.7 = ((f32[64,1,512]{2,1,0:T(1,128)}), f32[64,1,512]{2,1,0:T(1,128)S(1)}, u32[]{:S(2)}, u32[]{:S(2)}) async-start(f32[64,1,512]{2,1,0:T(1,128)} %reshape.189), calls=%async_computation.7 | async-start | bytes 262144 | tf_op jit(solution)/shard_map/all_to_all | solution.py:71
  333.5 16.9 %all-to-all-start.8 = ((bf16[64,2,256]{2,1,0:T(2,128)(2,1)}), bf16[64,2,256]{2,1,0:T(2,128)(2,1)S(1)}, u32[]{:S(2)}, u32[]{:S(2)}) async-start(bf16[64,2,256]{2,1,0:T(2,128)(2,1)} %reshape.191), calls=%async_computation.8 | async-start | bytes 131072 | tf_op jit(solution)/shard_map/all_to_all | solution.py:53
  (3 other events, 2.1 us)
where the time goes:
time: 352 us; the launch traced here: 351 us
  blocking collectives  208 us (59%)
  waiting for transfers between devices  67.3 us (19%)
  starting transfers between devices  45.8 us (13%)
  local copies, waits for them, and re-layouts  16.8 us (5%)
  other arithmetic  7.6 us (2%)
  matrix products  4.45 us (1%)
    psum x8, blocking collectives, over_axes(): shard = lax.psum(shard, axis)  104 us
    all_gather x2, blocking collectives, gather_turned(): lax.all_gather(both, axis, axis=0, tiled=True)  104 us
    all_to_all x5, waiting for transfers between devices, copy_for_each(): lax.all_to_all(jnp.broadcast_to(shard[None], (size, *shard.shape)), axis,...  33 us
    all_to_all x5, starting transfers between devices, copy_for_each(): lax.all_to_all(jnp.broadcast_to(shard[None], (size, *shard.shape)), axis,...  24.4 us
    all_to_all x2, waiting for transfers between devices, summed_on_arrival_2(): lax.all_to_all(pieces, axis, split_axis=0, concat_axis=0, tiled=True)  23.2 us
    all_to_all x2, starting transfers between devices, summed_on_arrival_2(): lax.all_to_all(pieces, axis, split_axis=0, concat_axis=0, tiled=True)  14.7 us
    all_to_all x2, waiting for transfers between devices, summed_on_arrival(): pieces = lax.all_to_all(cut_along(shard, dim, size), axis, 0, 0, tiled=True)  11.1 us
    unnamed x52, local copies, waits for them, and re-layouts  9.87 us
  transfers between devices with their start and end apart: 9, of which 9 were waited for; matrix products, arithmetic and copies ran while one was open for 1% of the time, Pallas kernels for 0%

commit v1 on v0

--- a/solution.py
+++ b/solution.py
@@ -11,6 +11,12 @@
 TP = ("tp_0", "tp_1")
 TP_DP = ("tp_0", "tp_1", "dp_0", "dp_1")
 eps = 1e-06
+
+
+def summed_here(block, name):
+    blocks = lax.all_gather(block, name, axis=0, tiled=False)
+    total = blocks.sum(axis=0)
+    return total
 
 
 def cut_along(shard, dim, size):
@@ -44,7 +50,7 @@
 
 def over_axes(shard, axes):
     for axis in axes:
-        shard = lax.psum(shard, axis)
+        shard = summed_here(shard, axis)
     return shard
 
 

time: 352 us -> 390 us (1.11)
  blocking collectives: 208 us -> 244 us
  waiting for transfers between devices: 67.3 us -> 59.8 us
  local copies, waits for them, and re-layouts: 16.8 us -> 23.1 us
    psum x8 -> x0, blocking collectives: 104 us -> none  [over_axes(): shard = lax.psum(shard, axis)]
    all_gather x0 -> x4, blocking collectives: none -> 98.5 us  [summed_here(): blocks = lax.all_gather(block, name, axis=0, tiled=False)]
    unnamed x0 -> x4, blocking collectives: none -> 41.5 us
    all_to_all x2, waiting for transfers between devices: 23.2 us -> 15.5 us  [summed_on_arrival_2(): lax.all_to_all(pieces, axis, split_axis=0, concat_axis=0, tiled=True)]
    unnamed x52 -> x64, local copies, waits for them, and re-layouts: 9.87 us -> 15.9 us
  transfers between devices with their start and end apart: 9 -> 9, of which waited for: 9 -> 9; matrix products, arithmetic and copies ran while one was open for 1% -> 2% of each run, Pallas kernels for 0% -> 0%
where the time goes in v1:
time: 390 us; the launch traced here: 389 us
  blocking collectives  244 us (63%)
  waiting for transfers between devices  59.8 us (15%)
  starting transfers between devices  45.8 us (12%)
  local copies, waits for them, and re-layouts  23.1 us (6%)
  other arithmetic  7.74 us (2%)
  matrix products  4.45 us (1%)
  between operations  3.9 us (1%)
    all_gather x2, blocking collectives, gather_turned(): lax.all_gather(both, axis, axis=0, tiled=True)  104 us
    all_gather x4, blocking collectives, summed_here(): blocks = lax.all_gather(block, name, axis=0, tiled=False)  98.5 us
    unnamed x4, blocking collectives  41.5 us
    all_to_all x5, waiting for transfers between devices, copy_for_each(): lax.all_to_all(jnp.broadcast_to(shard[None], (size, *shard.shape)), axis,...  33.3 us
    all_to_all x5, starting transfers between devices, copy_for_each(): lax.all_to_all(jnp.broadcast_to(shard[None], (size, *shard.shape)), axis,...  24.4 us
    unnamed x64, local copies, waits for them, and re-layouts  15.9 us
    all_to_all x2, waiting for transfers between devices, summed_on_arrival_2(): lax.all_to_all(pieces, axis, split_axis=0, concat_axis=0, tiled=True)  15.5 us
    all_to_all x2, starting transfers between devices, summed_on_arrival_2(): lax.all_to_all(pieces, axis, split_axis=0, concat_axis=0, tiled=True)  14.7 us
  transfers between devices with their start and end apart: 9, of which 9 were waited for; matrix products, arithmetic and copies ran while one was open for 2% of the time, Pallas kernels for 0%

profile of v1, /device:TPU:8, one launch (start us, length us, event | category | flops | bytes accessed | tf_op | source)
XLA Modules:
  0.0 388.6 jit_solution(14166485167418932632)
XLA Ops:
  2.3 4.4 %all-to-all-start = ((f32[8,64,1]{1,2,0:T(1,128)}), f32[8,64,1]{1,2,0:T(1,128)S(1)}, u32[]{:S(2)}, u32[]{:S(2)}) async-start(f32[8,64,1]{1,2,0:T(1,128)} %broadcast_in_dim.22), calls=%async_computation | async-start | bytes 8192 | tf_op jit(solution)/shard_map/all_to_all | solution.py:59
  16.0 3.4 all-to-all-start.1
  19.4 5.5 %all-to-all-done.1 = bf16[8,8,448]{2,1,0:T(8,128)(2,1)S(1)} async-done(((bf16[8,8,448]{2,1,0:T(8,128)(2,1)}), bf16[8,8,448]{2,1,0:T(8,128)(2,1)S(1)}, u32[]{:S(2)}, u32[]{:S(2)}) %all-to-all-start.1) | async-done | bytes 57376 | tf_op jit(solution)/shard_map/all_to_all | solution.py:29
  25.2 56.1 %all-gather.6 = bf16[64,32,16]{1,2,0:T(8,128)(2,1)S(1)} all-gather(bf16[1,32,16]{1,2,0:T(8,128)(2,1)S(1)} %maximum_bitcast_fusion), channel_id=1, replica_groups=mesh['tp_0'=8,'tp_1'=8,'dp_0'=4,'dp_1'=2] {'tp_0','tp_1'}, dimensions={0}, use_global_device_ids=true | all-gather | bytes 66560 | tf_op jit(solution)/shard_map/all_gather | solution.py:43
  84.0 24.7 %all_gather.48 = f32[8,8,16]{2,1,0:T(8,128)S(1)} all-gather(f32[1,8,16]{2,1,0:T(8,128)S(1)} %broadcast_multiply_fusion.3), channel_id=1, replica_groups=mesh['tp_0'=8,'tp_1'=8,'dp_0'=4,'dp_1'=2] {'tp_0'}, dimensions={0}, use_global_device_ids=true | all-gather | bytes 4608 | tf_op jit(solution)/shard_map/all_gather | solution.py:17
  108.7 24.5 %all-gather = f32[64,16]{1,0:T(8,128)S(1)} all-gather(f32[8,16]{1,0:T(8,128)S(1)} %reduce_sum.247), channel_id=2, replica_groups=mesh['tp_0'=8,'tp_1'=8,'dp_0'=4,'dp_1'=2] {'tp_1'}, dimensions={0}, use_global_device_ids=true | all-gather | bytes 4608 | tf_op jit(solution)/shard_map/all_gather | solution.py:17
  137.5 5.1 %all-to-all-done.2 = bf16[8,8,128]{2,1,0:T(8,128)(2,1)S(1)} async-done(((bf16[8,8,128]{2,1,0:T(8,128)(2,1)}), bf16[8,8,128]{2,1,0:T(8,128)(2,1)S(1)}, u32[]{:S(2)}, u32[]{:S(2)}) %all-to-all-start.2) | async-done | bytes 16416 | tf_op jit(solution)/shard_map/all_to_all | solution.py:59
  143.9 8.3 %all-to-all-start.3 = ((f32[64,1,512]{2,1,0:T(1,128)}), f32[64,1,512]{2,1,0:T(1,128)S(1)}, u32[]{:S(2)}, u32[]{:S(2)}) async-start(f32[64,1,512]{2,1,0:T(1,128)} %reshape.312), calls=%async_computation.3 | async-start | bytes 262144 | tf_op jit(solution)/shard_map/all_to_all | solution.py:77
  160.0 4.0 %all-to-all-done.3 = f32[64,1,512]{2,1,0:T(1,128)S(1)} async-done(((f32[64,1,512]{2,1,0:T(1,128)}), f32[64,1,512]{2,1,0:T(1,128)S(1)}, u32[]{:S(2)}, u32[]{:S(2)}) %all-to-all-start.3) | async-done | bytes 131104 | tf_op jit(solution)/shard_map/all_to_all | solution.py:77
  166.1 14.7 %all-reduce = f32[512]{0:T(512)S(1)} all-reduce(f32[512]{0:T(512)S(1)} %dynamic-update-slice), channel_id=3, replica_groups=mesh['tp_0'=8,'tp_1'=8,'dp_0'=4,'dp_1'=2] {'tp_0'}, use_global_device_ids=true, to_apply=%add | all-reduce | flops 512 | bytes 4096
  181.2 15.4 %all-reduce.1 = f32[512]{0:T(512)S(1)} all-reduce(f32[512]{0:T(512)S(1)} %dynamic-update-slice.1), channel_id=4, replica_groups=mesh['tp_0'=8,'tp_1'=8,'dp_0'=4,'dp_1'=2] {'tp_1'}, use_global_device_ids=true, to_apply=%add.1 | all-reduce | flops 512 | bytes 4096
  197.0 8.9 %all-reduce.2 = f32[256]{0:T(256)S(1)} all-reduce(f32[256]{0:T(256)S(1)} %dynamic-update-slice.2), channel_id=5, replica_groups=mesh['tp_0'=8,'tp_1'=8,'dp_0'=4,'dp_1'=2] {'dp_0'}, use_global_device_ids=true, to_apply=%add.2 | all-reduce | flops 256 | bytes 2048
  209.6 7.9 %all-to-all-start.4 = ((bf16[64,2,256]{2,1,0:T(2,128)(2,1)}), bf16[64,2,256]{2,1,0:T(2,128)(2,1)S(1)}, u32[]{:S(2)}, u32[]{:S(2)}) async-start(bf16[64,2,256]{2,1,0:T(2,128)(2,1)} %reshape.314), calls=%async_computation.4 | async-start | bytes 131072 | tf_op jit(solution)/shard_map/all_to_all | solution.py:59
  217.7 11.2 %all-to-all-done.4 = bf16[64,2,256]{2,1,0:T(2,128)(2,1)S(1)} async-done(((bf16[64,2,256]{2,1,0:T(2,128)(2,1)}), bf16[64,2,256]{2,1,0:T(2,128)(2,1)S(1)}, u32[]{:S(2)}, u32[]{:S(2)}) %all-to-all-start.4) | async-done | bytes 65568 | tf_op jit(solution)/shard_map/all_to_all | solution.py:59
  230.9 3.4 all-to-all-start.5
  234.3 5.5 %all-to-all-done.5 = bf16[8,8,448]{2,1,0:T(8,128)(2,1)S(1)} async-done(((bf16[8,8,448]{2,1,0:T(8,128)(2,1)}), bf16[8,8,448]{2,1,0:T(8,128)(2,1)S(1)}, u32[]{:S(2)}, u32[]{:S(2)}) %all-to-all-start.5) | async-done | bytes 57376 | tf_op jit(solution)/shard_map/all_to_all | solution.py:29
  240.2 47.8 %all-gather.7 = bf16[64,32,16]{1,2,0:T(8,128)(2,1)S(1)} all-gather(bf16[1,32,16]{1,2,0:T(8,128)(2,1)S(1)} %maximum_bitcast_fusion.1), channel_id=1, replica_groups=mesh['tp_0'=8,'tp_1'=8,'dp_0'=4,'dp_1'=2] {'tp_0','tp_1'}, dimensions={0}, use_global_device_ids=true | all-gather | bytes 66560 | tf_op jit(solution)/shard_map/all_gather | solution.py:43
  290.6 24.7 %all_gather.59 = f32[8,8,16]{2,1,0:T(8,128)S(1)} all-gather(f32[1,8,16]{2,1,0:T(8,128)S(1)} %broadcast_multiply_fusion.2), channel_id=1, replica_groups=mesh['tp_0'=8,'tp_1'=8,'dp_0'=4,'dp_1'=2] {'tp_0'}, dimensions={0}, use_global_device_ids=true | all-gather | bytes 4608 | tf_op jit(solution)/shard_map/all_gather | solution.py:17
  315.3 24.7 %all-gather.5 = f32[64,16]{1,0:T(8,128)S(1)} all-gather(f32[8,16]{1,0:T(8,128)S(1)} %reduce_sum.264), channel_id=7, replica_groups=mesh['tp_0'=8,'tp_1'=8,'dp_0'=4,'dp_1'=2] {'tp_1'}, dimensions={0}, use_global_device_ids=true | all-gather | bytes 4608 | tf_op jit(solution)/shard_map/all_gather | solution.py:17
  346.0 3.5 all-to-all-done.6
  350.7 6.4 %all-to-all-start.7 = ((f32[64,1,512]{2,1,0:T(1,128)}), f32[64,1,512]{2,1,0:T(1,128)S(1)}, u32[]{:S(2)}, u32[]{:S(2)}) async-start(f32[64,1,512]{2,1,0:T(1,128)} %reshape.316), calls=%async_computation.7 | async-start | bytes 262144 | tf_op jit(solution)/shard_map/all_to_all | solution.py:77
  357.4 11.4 %all-to-all-done.7 = f32[64,1,512]{2,1,0:T(1,128)S(1)} async-done(((f32[64,1,512]{2,1,0:T(1,128)}), f32[64,1,512]{2,1,0:T(1,128)S(1)}, u32[]{:S(2)}, u32[]{:S(2)}) %all-to-all-start.7) | async-done | bytes 131104 | tf_op jit(solution)/shard_map/all_to_all | solution.py:77
  370.9 5.4 %all-to-all-start.8 = ((bf16[64,2,256]{2,1,0:T(2,128)(2,1)}), bf16[64,2,256]{2,1,0:T(2,128)(2,1)S(1)}, u32[]{:S(2)}, u32[]{:S(2)}) async-start(bf16[64,2,256]{2,1,0:T(2,128)(2,1)} %reshape.318), calls=%async_computation.8 | async-start | bytes 131072 | tf_op jit(solution)/shard_map/all_to_all | solution.py:59
  377.3 10.5 %all-to-all-done.8 = bf16[64,2,256]{2,1,0:T(2,128)(2,1)S(1)} async-done(((bf16[64,2,256]{2,1,0:T(2,128)(2,1)}), bf16[64,2,256]{2,1,0:T(2,128)(2,1)S(1)}, u32[]{:S(2)}, u32[]{:S(2)}) %all-to-all-start.8) | async-done | bytes 65568 | tf_op jit(solution)/shard_map/all_to_all | solution.py:59
  (193 shorter events, 47.4 us)
Async XLA Ops:
  2.3 4.4 %copy-start.14 = (f32[2,2]{1,0:T(2,128)S(1)}, f32[2,2]{1,0:T(2,128)}, u32[]{:S(2)}) copy-start(f32[2,2]{1,0:T(2,128)} %param.31) | copy-start | bytes 52
  2.3 4.5 %copy-start.15 = (f32[2,128]{1,0:T(2,128)S(1)}, f32[2,128]{1,0:T(2,128)}, u32[]{:S(2)}) copy-start(f32[2,128]{1,0:T(2,128)} %param.32) | copy-start | bytes 3076
  2.3 9.6 %all-to-all-start = ((f32[8,64,1]{1,2,0:T(1,128)}), f32[8,64,1]{1,2,0:T(1,128)S(1)}, u32[]{:S(2)}, u32[]{:S(2)}) async-start(f32[8,64,1]{1,2,0:T(1,128)} %broadcast_in_dim.22), calls=%async_computation | async-start | bytes 8192 | tf_op jit(solution)/shard_map/all_to_all | solution.py:59
  6.7 0.7 copy-start.12
  7.4 0.7 copy-start.7
  8.1 0.7 copy-start.8
  8.1 0.7 copy-start.9
  8.1 0.7 copy-start.16
  8.1 0.7 copy-start.17
  8.2 3.8 copy-start.6
  11.9 0.8 copy-start.5
  12.0 1.2 copy-start.3
  13.0 1.0 copy-start.2
  14.0 0.9 copy-start.4
  16.0 8.9 %all-to-all-start.1 = ((bf16[8,8,448]{2,1,0:T(8,128)(2,1)}), bf16[8,8,448]{2,1,0:T(8,128)(2,1)S(1)}, u32[]{:S(2)}, u32[]{:S(2)}) async-start(bf16[8,8,448]{2,1,0:T(8,128)(2,1)} %bitcast.6), calls=%async_computation.1 | async-start | bytes 131072 | tf_op jit(solution)/shard_map/all_to_all | solution.py:29
  81.3 1.5 copy-start
  83.6 53.7 %copy-start.1 = (bf16[2,128,512]{2,1,0:T(8,128)(2,1)S(1)}, bf16[2,128,512]{2,1,0:T(8,128)(2,1)}, u32[]{:S(2)}) copy-start(bf16[2,128,512]{2,1,0:T(8,128)(2,1)} %param.33) | copy-start | bytes 786436
  134.0 8.6 %all-to-all-start.2 = ((bf16[8,8,128]{2,1,0:T(8,128)(2,1)}), bf16[8,8,128]{2,1,0:T(8,128)(2,1)S(1)}, u32[]{:S(2)}, u32[]{:S(2)}) async-start(bf16[8,8,128]{2,1,0:T(8,128)(2,1)} %broadcast_in_dim.26), calls=%async_computation.2 | async-start | bytes 32768 | tf_op jit(solution)/shard_map/all_to_all | solution.py:59
  143.9 20.2 %all-to-all-start.3 = ((f32[64,1,512]{2,1,0:T(1,128)}), f32[64,1,512]{2,1,0:T(1,128)S(1)}, u32[]{:S(2)}, u32[]{:S(2)}) async-start(f32[64,1,512]{2,1,0:T(1,128)} %reshape.312), calls=%async_computation.3 | async-start | bytes 262144 | tf_op jit(solution)/shard_map/all_to_all | solution.py:77
  209.6 19.2 %all-to-all-start.4 = ((bf16[64,2,256]{2,1,0:T(2,128)(2,1)}), bf16[64,2,256]{2,1,0:T(2,128)(2,1)S(1)}, u32[]{:S(2)}, u32[]{:S(2)}) async-start(bf16[64,2,256]{2,1,0:T(2,128)(2,1)} %reshape.314), calls=%async_computation.4 | async-start | bytes 131072 | tf_op jit(solution)/shard_map/all_to_all | solution.py:59
  230.9 8.9 %all-to-all-start.5 = ((bf16[8,8,448]{2,1,0:T(8,128)(2,1)}), bf16[8,8,448]{2,1,0:T(8,128)(2,1)S(1)}, u32[]{:S(2)}, u32[]{:S(2)}) async-start(bf16[8,8,448]{2,1,0:T(8,128)(2,1)} %bitcast.48), calls=%async_computation.5 | async-start | bytes 131072 | tf_op jit(solution)/shard_map/all_to_all | solution.py:29
  340.8 8.6 %all-to-all-start.6 = ((bf16[8,8,128]{2,1,0:T(8,128)(2,1)}), bf16[8,8,128]{2,1,0:T(8,128)(2,1)S(1)}, u32[]{:S(2)}, u32[]{:S(2)}) async-start(bf16[8,8,128]{2,1,0:T(8,128)(2,1)} %broadcast_in_dim.31), calls=%async_computation.6 | async-start | bytes 32768 | tf_op jit(solution)/shard_map/all_to_all | solution.py:59
  350.7 18.2 %all-to-all-start.7 = ((f32[64,1,512]{2,1,0:T(1,128)}), f32[64,1,512]{2,1,0:T(1,128)S(1)}, u32[]{:S(2)}, u32[]{:S(2)}) async-start(f32[64,1,512]{2,1,0:T(1,128)} %reshape.316), calls=%async_computation.7 | async-start | bytes 262144 | tf_op jit(solution)/shard_map/all_to_all | solution.py:77
  370.9 16.9 %all-to-all-start.8 = ((bf16[64,2,256]{2,1,0:T(2,128)(2,1)}), bf16[64,2,256]{2,1,0:T(2,128)(2,1)S(1)}, u32[]{:S(2)}, u32[]{:S(2)}) async-start(bf16[64,2,256]{2,1,0:T(2,128)(2,1)} %reshape.318), calls=%async_computation.8 | async-start | bytes 131072 | tf_op jit(solution)/shard_map/all_to_all | solution.py:59
  (3 other events, 2.1 us)
